TPU v7x, 32 devices: a whole 2x2x4 slice. The times are simulated.
32 devices in a mesh: grp: 2 (over y), sp: 4 (over z), tp: 4 (over x, core).
Axes of the slice: x: 2, y: 2, z: 4, core: 2. Of those that a mesh axis runs over, the one named last changes fastest.
Arguments:
- residual_in: bfloat16 [2048, 2048], P(('grp', 'sp', 'tp')), parts along dimension 0, may hold values from -6 to 6
- query_rows: bfloat16 [2048, 2048], P(('grp', 'sp'), 'tp'), parts along dimension 0, may hold values from -6 to 6
- key_rows: bfloat16 [2048, 512], P(('grp', 'sp'), 'tp'), parts along dimension 0, may hold values from -6 to 6
- value_rows: bfloat16 [2048, 512], P(('grp', 'sp'), 'tp'), parts along dimension 0, may hold values from -6 to 6
- forget_cumsum: float32 [2048, 16], P(('grp', 'sp'), 'tp'), parts along dimension 0, as said below
- head_gain: float32 [2048], P('tp'), may hold values from 0.1 to 1.9
- w_out: bfloat16 [2048, 2048], P('tp'), may hold values from -0.125 to 0.125
- w_up: bfloat16 [2048, 8192], P('sp', 'tp'), may hold values from -0.125 to 0.125
- w_down: bfloat16 [8192, 2048], P('tp', 'sp'), may hold values from -0.0625 to 0.0625
- mixer_gain: float32 [2048], replicated, may hold values from 0.1 to 1.9
- channel_gain: float32 [2048], replicated, may hold values from 0.1 to 1.9
Outputs:
- layer_out: bfloat16 [2048, 2048], P(('grp', 'sp', 'tp')), parts along dimension 0
There are 2 independent parts, one for each index of `grp`. A program takes and returns all parts, laid end to end along the dimension named above; an argument that names none is the same for every part. Nothing has to cross between parts.
Inputs may be any that keep to these rules, and one draw needn't show every extreme that they name: `forget_cumsum`: Non-positive; along the positions, each head's entries never rise.
All inputs are finite; a program needn't handle non-finite values.
Results may differ from a plain program's by a relative error of at most 0.015.
Values may be sent and summed in bfloat16 or wider, within the bound.
A program may use at most 128 MiB of HBM per device.

v0:
```python
import jax
import jax.numpy as jnp
from jax import lax
from jax.sharding import PartitionSpec as P

HD = 128


ALPHA = 8.0**0.25
EPSILON = 1e-05
NEG_FILL = -1e30


def layer_scale(inputs, gain_vec):
    centered = inputs - jnp.mean(inputs, axis=-1, keepdims=True)
    variance = jnp.mean(centered * centered, axis=-1, keepdims=True)
    return centered * lax.rsqrt(variance + EPSILON) * gain_vec


def shards(
    residual_in,
    query_rows,
    key_rows,
    value_rows,
    forget_cumsum,
    head_gain,
    w_out,
    w_up,
    w_down,
    mixer_gain,
    channel_gain,
):
    tok_rows = query_rows.shape[0]
    heads_here = forget_cumsum.shape[1]
    kv_here = key_rows.shape[1] // HD
    group_size = heads_here // kv_here
    score_scale = HD ** (-0.5)
    seq_index = lax.axis_index("sp")
    gate_all = lax.all_gather(forget_cumsum, "sp", axis=0, tiled=True)
    query_grid = query_rows.reshape(tok_rows, kv_here, group_size, HD)
    query_pos = seq_index * tok_rows + jnp.arange(tok_rows, dtype=jnp.int32)
    last_query = seq_index * tok_rows + tok_rows - 1
    gate_query = forget_cumsum.reshape(tok_rows, kv_here, group_size).transpose(1, 2, 0)

    def attend(carry_state, key_block, value_block, first_row):
        row_count = key_block.shape[0]

        def attend_live(live_state):
            peak_score, denom_sum, accum = live_state
            key_grid = key_block.reshape(row_count, kv_here, HD)
            value_grid = value_block.reshape(row_count, kv_here, HD)
            gate_block = lax.dynamic_slice_in_dim(gate_all, first_row, row_count, 0)
            gate_block = gate_block.reshape(row_count, kv_here, group_size).transpose(1, 2, 0)
            scores = (
                jnp.einsum(
                    "tkgd,ukd->kgtu", query_grid, key_grid, preferred_element_type=jnp.float32
                )
                * score_scale
            )
            scores = scores + gate_query[..., None] - gate_block[:, :, None, :]
            key_pos = first_row + jnp.arange(row_count, dtype=jnp.int32)
            allowed = key_pos[None, :] <= query_pos[:, None]
            scores = jnp.where(allowed, scores, NEG_FILL)
            new_peak = jnp.maximum(peak_score, jnp.max(scores, axis=-1))
            weights = jnp.where(allowed, jnp.exp(scores - new_peak[..., None]), 0.0)
            fade_factor = jnp.exp(peak_score - new_peak)
            denom_sum = denom_sum * fade_factor + jnp.sum(weights, axis=-1)
            accum = accum * fade_factor[..., None] + jnp.einsum(
                "kgtu,ukd->kgtd",
                weights.astype(jnp.bfloat16),
                value_grid,
                preferred_element_type=jnp.float32,
            )
            return (new_peak, denom_sum, accum)

        return lax.cond(
            first_row <= last_query, attend_live, lambda kept_state: kept_state, carry_state
        )

    def fold_keys(carry_state, pieces, first_row):
        key_piece, value_piece = pieces
        row_count = key_piece.shape[0]
        block_span = 1024
        if row_count > block_span and row_count % block_span == 0:

            def scan_block(scan_state, block_index):
                offset = block_index * block_span
                next_state = attend(
                    scan_state,
                    lax.dynamic_slice_in_dim(key_piece, offset, block_span, 0),
                    lax.dynamic_slice_in_dim(value_piece, offset, block_span, 0),
                    first_row + offset,
                )
                return (next_state, None)

            carry_state, unused = lax.scan(
                scan_block, carry_state, jnp.arange(row_count // block_span, dtype=jnp.int32)
            )
            return carry_state
        return attend(carry_state, key_piece, value_piece, first_row)

    fold_init = (
        jnp.full((kv_here, group_size, tok_rows), NEG_FILL, jnp.float32),
        jnp.zeros((kv_here, group_size, tok_rows), jnp.float32),
        jnp.zeros((kv_here, group_size, tok_rows, HD), jnp.float32),
    )
    peak_score, denom_sum, accum = fold_keys(
        fold_init,
        (
            lax.all_gather(key_rows, "sp", axis=0, tiled=True),
            lax.all_gather(value_rows, "sp", axis=0, tiled=True),
        ),
        jnp.int32(0),
    )
    attended = accum / denom_sum[..., None]
    normed = attended * lax.rsqrt(jnp.mean(attended * attended, axis=-1, keepdims=True) + EPSILON)
    normed = normed * head_gain.reshape(kv_here, group_size, 1, HD)
    heads_out = normed.transpose(2, 0, 1, 3).reshape(tok_rows, heads_here * HD).astype(jnp.bfloat16)
    branch = lax.psum_scatter(
        jnp.dot(heads_out, w_out, preferred_element_type=jnp.float32).astype(jnp.bfloat16),
        "tp",
        scatter_dimension=0,
        tiled=True,
    ).astype(jnp.float32)
    mid_rows = layer_scale(ALPHA * residual_in.astype(jnp.float32) + branch, mixer_gain).astype(
        jnp.bfloat16
    )
    mid_all = lax.all_gather(mid_rows, "tp", axis=0, tiled=True)
    up_full, down_full = (
        lax.all_gather(w_up, "sp", axis=0, tiled=True),
        lax.all_gather(w_down, "sp", axis=1, tiled=True),
    )
    lifted = jnp.dot(mid_all, up_full, preferred_element_type=jnp.float32)
    active = jnp.square(jax.nn.relu(lifted)).astype(jnp.bfloat16)
    lowered = lax.psum_scatter(
        jnp.dot(active, down_full, preferred_element_type=jnp.float32).astype(jnp.bfloat16),
        "tp",
        scatter_dimension=0,
        tiled=True,
    ).astype(jnp.float32)
    return layer_scale(ALPHA * mid_rows.astype(jnp.float32) + lowered, channel_gain).astype(
        jnp.bfloat16
    )


def solution(mesh):
    placed = (
        P(("grp", "sp", "tp"), None),
        P(("grp", "sp"), "tp"),
        P(("grp", "sp"), "tp"),
        P(("grp", "sp"), "tp"),
        P(("grp", "sp"), "tp"),
        P("tp"),
        P("tp", None),
        P("sp", "tp"),
        P("tp", "sp"),
        P(),
        P(),
    )
    return jax.shard_map(
        shards, mesh=mesh, in_specs=placed, out_specs=P(("grp", "sp", "tp"), None), check_vma=False
    )
```

profile of v0, /device:TPU:0, one launch (start us, length us, event | category | flops | bytes accessed | tf_op | source)
XLA Modules:
  0.0 451.6 jit_solution(16163317256759813407)
XLA Ops:
  6.5 16.0 %all_gather.18 = bf16[1024,128]{1,0:T(8,128)(2,1)S(1)} all-gather(bf16[256,128]{1,0:T(8,128)(2,1)} %param.15), channel_id=1, replica_groups=mesh['grp'=2,'sp'=4,'tp'=4] {'sp'}, dimensions={0}, use_global_device_ids=true | all-gather | bytes 327680 | tf_op jit(solution)/shard_map/all_gather | solution.py:110
  22.5 14.8 %all_gather.20 = bf16[1024,128]{1,0:T(8,128)(2,1)S(1)} all-gather(bf16[256,128]{1,0:T(8,128)(2,1)} %param.16), channel_id=1, replica_groups=mesh['grp'=2,'sp'=4,'tp'=4] {'sp'}, dimensions={0}, use_global_device_ids=true | all-gather | bytes 327680 | tf_op jit(solution)/shard_map/all_gather | solution.py:111
  37.4 13.3 %all_gather.19 = f32[1024,4]{0,1:T(4,128)S(1)} all-gather(f32[256,4]{0,1:T(4,128)} %param.17), channel_id=1, replica_groups=mesh['grp'=2,'sp'=4,'tp'=4] {'sp'}, dimensions={0}, use_global_device_ids=true | all-gather | bytes 20480 | tf_op jit(solution)/shard_map/all_gather | solution.py:39
  50.7 6.1 %conditional.1 = (f32[1,4,256]{2,1,0:T(4,128)S(1)}, f32[1,4,256,128]{2,3,1,0:T(8,128)S(1)}) conditional(s32[]{:T(128)} %convert_element_type.43, () %tuple.13, (s32[]{:T(128)}, s32[256]{0:T(256)S(1)}, bf16[256,512]{1,0:T(8,128)(2,1)}, bf16[1024,128]{1,0:T(8,128)(2,1)S(1)}, f32[1,4,256]{2,1,0:T(4,128)}, /*index=5*/f32[1024,4]{0,1:T(4,128)S(1)}, ...), branch_computations={%region_0.0_spmd, %region_1.4_spmd} | conditional | flops 557190400 | bytes 16116784 | solution.py:76
  50.7 0.2 iota_compare_fusion
  50.9 2.1 fusion.4
  53.0 1.5 fusion.3
  54.5 2.1 fusion.12
  56.6 0.2 copy.20
  57.1 1.7 convolution_convert_fusion
  58.9 25.8 %reduce-scatter.3.cloned.1.call-done = bf16[64,2048]{1,0:T(8,128)(2,1)} async-done(((bf16[256,2048]{1,0:T(8,128)(2,1)}), bf16[64,2048]{1,0:T(8,128)(2,1)}) %reduce-scatter.3.cloned.1.call-update) | async-done | bytes 262160 | tf_op jit(solution)/shard_map/reduce_scatter | solution.py:119
  84.7 1.1 fusion.25
  85.9 1.2 multiply_reduce_fusion.1
  87.1 1.8 multiply_convert_fusion.1
  88.9 0.7 all-gather.6.cloned.1.call-update
  89.7 0.5 all-gather.8.cloned.1.call-update
  90.3 15.5 %all-gather.4.cloned.1.call-done = bf16[256,2048]{1,0:T(8,128)(2,1)} async-done(((bf16[64,2048]{1,0:T(8,128)(2,1)}), bf16[256,2048]{1,0:T(8,128)(2,1)}) %all-gather.4.cloned.1.call-update) | async-done | bytes 1048592 | tf_op jit(solution)/shard_map/all_gather | solution.py:128
  105.7 151.2 %all-gather.6.cloned.1.call-done = bf16[2048,2048]{1,0:T(8,128)(2,1)} async-done(((bf16[512,2048]{1,0:T(8,128)(2,1)}), bf16[2048,2048]{1,0:T(8,128)(2,1)}) %all-gather.6.cloned.1.call-update) | async-done | bytes 8388624 | tf_op jit(solution)/shard_map/all_gather | solution.py:130
  257.0 149.3 %all-gather.8.cloned.1.call-done = bf16[2048,2048]{1,0:T(8,128)(2,1)} async-done(((bf16[2048,512]{1,0:T(8,128)(2,1)}), bf16[2048,2048]{1,0:T(8,128)(2,1)}) %all-gather.8.cloned.1.call-update) | async-done | bytes 8388624 | tf_op jit(solution)/shard_map/all_gather | solution.py:131
  406.2 11.6 %convolution_convert_fusion.1 = bf16[256,2048]{1,0:T(8,128)(2,1)} fusion(bf16[2048,2048]{1,0:T(8,128)(2,1)} %all-gather.8.cloned.1.call-done, bf16[256,2048]{1,0:T(8,128)(2,1)} %all-gather.4.cloned.1.call-done, bf16[2048,2048]{1,0:T(8,128)(2,1)} %all-gather.6.cloned.1.call-done), kind=kOutput, calls=%fused_computation.29 | convolution fusion | flops 4297064448 | bytes 18874368 | tf_op jit(solution)/shard_map/dot_general | solution.py:136
  417.8 23.1 %reduce-scatter.5.cloned.1.call-done = bf16[64,2048]{1,0:T(8,128)(2,1)} async-done(((bf16[256,2048]{1,0:T(8,128)(2,1)}), bf16[64,2048]{1,0:T(8,128)(2,1)}) %reduce-scatter.5.cloned.1.call-update) | async-done | bytes 262160 | tf_op jit(solution)/shard_map/reduce_scatter | solution.py:135
  440.9 1.1 fusion.26
  442.0 1.2 multiply_reduce_fusion
  443.2 1.8 multiply_convert_fusion
  (33 shorter events, 0.5 us)
Async XLA Ops:
  6.5 50.5 %copy-start = (bf16[512,2048]{1,0:T(8,128)(2,1)S(1)}, bf16[512,2048]{1,0:T(8,128)(2,1)}, u32[]{:S(2)}) copy-start(bf16[512,2048]{1,0:T(8,128)(2,1)} %param.19) | copy-start | bytes 6291460
  6.5 78.2 %reduce-scatter.3.cloned.1.call-start = ((), (), s32[]{:S(2)}) async-start(), calls=%async_computation.2 | async-start | bytes 1310720 | tf_op jit(solution)/shard_map/reduce_scatter | solution.py:119
  50.7 6.2 %copy-start.6 = (f32[512]{0:T(512)S(1)}, f32[512]{0:T(512)}, u32[]{:S(2)}) copy-start(f32[512]{0:T(512)} %param.18) | copy-start | bytes 6148
  50.7 2.3 copy-start.3
  56.8 27.9 %copy-start.2 = (bf16[64,2048]{1,0:T(8,128)(2,1)S(1)}, bf16[64,2048]{1,0:T(8,128)(2,1)}, u32[]{:S(2)}) copy-start(bf16[64,2048]{1,0:T(8,128)(2,1)} %param.13) | copy-start | bytes 786436
  56.8 30.2 %copy-start.4 = (f32[2048]{0:T(1024)S(1)}, f32[2048]{0:T(1024)}, u32[]{:S(2)}) copy-start(f32[2048]{0:T(1024)} %param.22) | copy-start | bytes 24580
  58.8 46.9 %all-gather.4.cloned.1.call-start = ((), (), s32[]{:S(2)}) async-start(), calls=%async_computation.3 | async-start | bytes 1310720 | tf_op jit(solution)/shard_map/all_gather | solution.py:128
  88.9 168.1 %all-gather.6.cloned.1.call-start = ((), (), s32[]{:S(2)}) async-start(), calls=%async_computation.4 | async-start | bytes 10485760 | tf_op jit(solution)/shard_map/all_gather | solution.py:130
  89.6 316.6 %all-gather.8.cloned.1.call-start = ((), (), s32[]{:S(2)}) async-start(), calls=%async_computation.5 | async-start | bytes 10485760 | tf_op jit(solution)/shard_map/all_gather | solution.py:131
  90.2 350.7 %copy-start.1 = (bf16[64,2048]{1,0:T(8,128)(2,1)S(1)}, bf16[64,2048]{1,0:T(8,128)(2,1)}, u32[]{:S(2)}) copy-start(bf16[64,2048]{1,0:T(8,128)(2,1)} %multiply_convert_fusion.1) | copy-start | bytes 786436
  90.2 353.0 %copy-start.5 = (f32[2048]{0:T(1024)S(1)}, f32[2048]{0:T(1024)}, u32[]{:S(2)}) copy-start(f32[2048]{0:T(1024)} %param.23) | copy-start | bytes 24580
  90.2 350.7 %reduce-scatter.5.cloned.1.call-start = ((), (), s32[]{:S(2)}) async-start(), calls=%async_computation.6 | async-start | bytes 1310720 | tf_op jit(solution)/shard_map/reduce_scatter | solution.py:135
Sparse Core Ops, SparseCore 0:
  59.0 25.7 reduce-scatter.2
  89.0 16.6 all-gather.3
  107.3 149.6 all-gather.5
  258.4 147.7 all-gather.7
  417.9 22.9 reduce-scatter.4
where the time goes:
time: 452 us
  waiting for transfers between devices  366 us (81%)
  blocking collectives  44.2 us (10%)
  matrix products  17.5 us (4%)
  between operations  13.3 us (3%)
  other arithmetic  10.1 us (2%)
    all_gather x1, waiting for transfers between devices, shards(): lax.all_gather(w_up, 'sp', axis=0, tiled=True)  151 us
    all_gather x1, waiting for transfers between devices, shards(): lax.all_gather(w_down, 'sp', axis=1, tiled=True)  149 us
    reduce_scatter x1, waiting for transfers between devices, shards(): lax.psum_scatter(jnp.dot(heads_out, w_out, preferred_element_type=jnp.flo...  25.8 us
    reduce_scatter x1, waiting for transfers between devices, shards(): lax.psum_scatter(jnp.dot(active, down_full, preferred_element_type=jnp.fl...  23.1 us
    all_gather x1, blocking collectives, shards(): lax.all_gather(key_rows, 'sp', axis=0, tiled=True)  16 us
    all_gather x1, waiting for transfers between devices, shards(): mid_all = lax.all_gather(mid_rows, 'tp', axis=0, tiled=True)  15.5 us
    all_gather x1, blocking collectives, shards(): lax.all_gather(value_rows, 'sp', axis=0, tiled=True)  14.8 us
    all_gather x1, blocking collectives, shards(): gate_all = lax.all_gather(forget_cumsum, 'sp', axis=0, tiled=True)  13.3 us
  transfers between devices with their start and end apart: 5, of which 5 were waited for; matrix products, arithmetic and copies ran while one was open for 0% of the time, Pallas kernels for 0%

commit v1 on v0

--- a/solution.py
+++ b/solution.py
@@ -1,7 +1,13 @@
+import functools
+
 import jax
 import jax.numpy as jnp
 from jax import lax
+from jax.experimental import pallas as pl
+from jax.experimental.pallas import tpu as pltpu
 from jax.sharding import PartitionSpec as P
+
+MESH = pl.DeviceIdType.MESH
 
 HD = 128
 
@@ -143,6 +149,530 @@
     )
 
 
+def layer_kernel(
+    G,
+    S,
+    T,
+    q_ref,
+    k_ref,
+    v_ref,
+    gq_ref,
+    gk_ref,
+    res_ref,
+    hg_ref,
+    mg_ref,
+    cg_ref,
+    wout_hbm,
+    wup_hbm,
+    wdn_hbm,
+    out_ref,
+    kbuf,
+    vbuf,
+    gbuf,
+    wout,
+    wup,
+    wdn,
+    heads_v,
+    mid_all,
+    act,
+    send_a,
+    recv_a,
+    keep,
+    send_b,
+    recv_b,
+    own,
+    send_c,
+    recv_c,
+    st_m,
+    st_l,
+    st_o,
+    kv_s,
+    kv_r,
+    wz_s,
+    wz_r,
+    wy_s,
+    wy_r,
+    loc,
+    z_s,
+    z_r,
+    x_s,
+    x_r,
+    d_s,
+    d_r,
+    a_s,
+    a_r,
+    b_s,
+    b_r,
+    c_s,
+    c_r,
+):
+    f32, bf16 = jnp.float32, jnp.bfloat16
+    X = T // 2
+    g, s, t = lax.axis_index("grp"), lax.axis_index("sp"), lax.axis_index("tp")
+    x, c = t // 2, lax.rem(t, 2)
+    mate = x * 2 + (1 - c)
+    tok = q_ref.shape[0]
+    heads = gq_ref.shape[1]
+    kv_heads = k_ref.shape[1] // HD
+    group = heads // kv_heads
+    rows = tok // T
+    half = X * rows
+    D = res_ref.shape[1]
+    dcut = D // S
+    fcut = wup.shape[1]
+
+    def remote(src, dst, ssem, rsem, **where):
+        return pltpu.make_async_remote_copy(
+            src_ref=src,
+            dst_ref=dst,
+            send_sem=ssem,
+            recv_sem=rsem,
+            device_id=where,
+            device_id_type=MESH,
+        )
+
+    def at_x(xo):
+        return xo * 2 + c
+
+    others_s = [lax.rem(s + d, S) for d in range(1, S)]
+    others_x = [lax.rem(x + d, X) for d in range(1, X)]
+    others_g = [lax.rem(g + d, G) for d in range(1, G)]
+
+    own_copies = [
+        pltpu.make_async_copy(wout_hbm, wout, loc.at[0]),
+        pltpu.make_async_copy(
+            wup_hbm.at[:, pl.ds(pl.multiple_of(s * fcut, fcut), fcut)],
+            wup.at[pl.ds(pl.multiple_of(s * dcut, dcut), dcut), :],
+            loc.at[1],
+        ),
+        pltpu.make_async_copy(
+            wdn_hbm.at[pl.ds(pl.multiple_of(s * fcut, fcut), fcut), :],
+            wdn.at[:, pl.ds(pl.multiple_of(s * dcut, dcut), dcut)],
+            loc.at[2],
+        ),
+    ]
+    for copy in own_copies:
+        copy.start()
+
+    barrier = pltpu.get_barrier_semaphore()
+    for so in others_s:
+        pl.semaphore_signal(barrier, inc=1, device_id={"sp": so}, device_id_type=MESH)
+    for xo in others_x:
+        pl.semaphore_signal(barrier, inc=1, device_id={"tp": at_x(xo)}, device_id_type=MESH)
+    pl.semaphore_signal(barrier, inc=1, device_id={"tp": mate}, device_id_type=MESH)
+    for go in others_g:
+        pl.semaphore_signal(barrier, inc=1, device_id={"grp": go}, device_id_type=MESH)
+    pl.semaphore_wait(barrier, (S - 1) + (X - 1) + 1 + (G - 1))
+
+    def kv_copies(d):
+        to = lax.rem(s + d, S)
+        return [
+            remote(k_ref, kbuf.at[d], kv_s.at[d, 0], kv_r.at[d, 0], sp=to),
+            remote(v_ref, vbuf.at[d], kv_s.at[d, 1], kv_r.at[d, 1], sp=to),
+            remote(gk_ref, gbuf.at[d], kv_s.at[d, 2], kv_r.at[d, 2], sp=to),
+        ]
+
+    for d in range(1, S):
+
+        @pl.when(s + d < S)
+        def _(d=d):
+            for copy in kv_copies(d):
+                copy.start()
+
+    uprow, dnrow = dcut // G, fcut // G
+
+    def up_piece(so, go):
+        return wup.at[pl.ds(pl.multiple_of(so * dcut + go * uprow, uprow), uprow), :]
+
+    def dn_piece(so, go):
+        return wdn.at[
+            pl.ds(pl.multiple_of(go * dnrow, dnrow), dnrow),
+            pl.ds(pl.multiple_of(so * dcut, dcut), dcut),
+        ]
+
+    def z_weight(m, to):
+        if m == 0:
+            src = wup_hbm.at[
+                pl.ds(pl.multiple_of(g * uprow, uprow), uprow),
+                pl.ds(pl.multiple_of(to * fcut, fcut), fcut),
+            ]
+            dst = up_piece(s, g)
+        else:
+            src = wdn_hbm.at[pl.ds(pl.multiple_of(to * fcut + g * dnrow, dnrow), dnrow), :]
+            dst = dn_piece(s, g)
+        return remote(src, dst, wz_s.at[m, to], wz_r.at[m, s], sp=to)
+
+    def z_weight_in(m, so):
+        dst = up_piece(so, g) if m == 0 else dn_piece(so, g)
+        return remote(dst, dst, wz_s.at[m, so], wz_r.at[m, so], sp=so)
+
+    def y_weight(m, so, go):
+        ref = up_piece(so, g) if m == 0 else dn_piece(so, g)
+        return remote(ref, ref, wy_s.at[m, so, go], wy_r.at[m, so, g], grp=go)
+
+    def y_weight_in(m, so, go):
+        ref = up_piece(so, go) if m == 0 else dn_piece(so, go)
+        return remote(ref, ref, wy_s.at[m, so, go], wy_r.at[m, so, go], grp=go)
+
+    def start_weight(m):
+        for so in others_s:
+            z_weight(m, so).start()
+
+    def forward_weight(m):
+        for so in others_s:
+            z_weight_in(m, so).wait_recv()
+            for go in others_g:
+                y_weight(m, so, go).start()
+
+    def finish_weight(m):
+        for so in others_s:
+            for go in others_g:
+                y_weight_in(m, so, go).wait_recv()
+
+    start_weight(0)
+    start_weight(1)
+
+    scale = HD ** (-0.5)
+    nt = (((1,), (1,)), ((), ()))
+    tri = lax.broadcasted_iota(jnp.int32, (tok, tok), 0) >= lax.broadcasted_iota(
+        jnp.int32, (tok, tok), 1
+    )
+    for h in range(heads):
+        kh = h // group
+        sc = lax.dot_general(
+            q_ref[:, h * HD : (h + 1) * HD],
+            k_ref[:, kh * HD : (kh + 1) * HD],
+            nt,
+            preferred_element_type=f32,
+        )
+        sc = sc * scale + gq_ref[:, h : h + 1] - gk_ref[h : h + 1, :]
+        sc = jnp.where(tri, sc, NEG_FILL)
+        peak = jnp.max(sc, axis=-1, keepdims=True)
+        w = jnp.where(tri, jnp.exp(sc - peak), 0.0)
+        st_m[h] = jnp.broadcast_to(peak, (tok, HD))
+        st_l[h] = jnp.broadcast_to(jnp.sum(w, axis=-1, keepdims=True), (tok, HD))
+        st_o[h] = jnp.dot(
+            w.astype(bf16), v_ref[:, kh * HD : (kh + 1) * HD], preferred_element_type=f32
+        )
+
+    def fold(j, carry):
+        @pl.when(s - j >= 0)
+        def _():
+            remote(k_ref, kbuf.at[j], kv_s.at[j, 0], kv_r.at[j, 0], sp=s).wait_recv()
+            remote(v_ref, vbuf.at[j], kv_s.at[j, 1], kv_r.at[j, 1], sp=s).wait_recv()
+            remote(gk_ref, gbuf.at[j], kv_s.at[j, 2], kv_r.at[j, 2], sp=s).wait_recv()
+            for h in range(heads):
+                kh = h // group
+                sc = lax.dot_general(
+                    q_ref[:, h * HD : (h + 1) * HD],
+                    kbuf[j, :, kh * HD : (kh + 1) * HD],
+                    nt,
+                    preferred_element_type=f32,
+                )
+                sc = sc * scale + gq_ref[:, h : h + 1] - gbuf[j, h : h + 1, :]
+                old = st_m[h][:, :1]
+                peak = jnp.maximum(old, jnp.max(sc, axis=-1, keepdims=True))
+                w = jnp.exp(sc - peak)
+                fade = jnp.exp(old - peak)
+                st_m[h] = jnp.broadcast_to(peak, (tok, HD))
+                st_l[h] = st_l[h] * fade + jnp.sum(w, axis=-1, keepdims=True)
+                st_o[h] = st_o[h] * fade + jnp.dot(
+                    w.astype(bf16),
+                    vbuf[j, :, kh * HD : (kh + 1) * HD],
+                    preferred_element_type=f32,
+                )
+
+        return carry
+
+    lax.fori_loop(1, S, fold, 0)
+
+    for h in range(heads):
+        a = st_o[h] / st_l[h]
+        a = a * lax.rsqrt(jnp.mean(a * a, axis=-1, keepdims=True) + EPSILON)
+        a = (a * hg_ref[:, h * HD : (h + 1) * HD]).astype(bf16)
+        for to in range(T):
+            heads_v[to % 2, (to // 2) * rows : (to // 2 + 1) * rows, h * HD : (h + 1) * HD] = a[
+                to * rows : (to + 1) * rows
+            ]
+
+    chunk = 512 if D % 512 == 0 else 128
+
+    def product(lhs, weight, put):
+        for n in range(0, D, chunk):
+            put(n, jnp.dot(lhs, weight[:, n : n + chunk], preferred_element_type=f32))
+
+    def copy_a(i):
+        return remote(send_a.at[i], recv_a.at[i], a_s.at[i], a_r.at[i], tp=mate)
+
+    def copy_b(i, xo):
+        return remote(
+            send_b.at[i, xo], recv_b.at[i, x], b_s.at[i, xo], b_r.at[i, x], tp=at_x(xo)
+        )
+
+    def copy_b_in(i, xo):
+        return remote(
+            send_b.at[i, xo], recv_b.at[i, xo], b_s.at[i, xo], b_r.at[i, xo], tp=at_x(xo)
+        )
+
+    def stage_a(i, lhs_of, weight):
+        def put_far(n, val):
+            send_a[i, :, n : n + chunk] = val.astype(bf16)
+
+        def put_near(n, val):
+            keep[i, :, n : n + chunk] = val
+
+        product(lhs_of(1 - c), weight, put_far)
+        copy_a(i).start()
+        product(lhs_of(c), weight, put_near)
+
+    def stage_b(i):
+        copy_a(i).wait_recv()
+        for xo in others_x:
+            at = pl.ds(pl.multiple_of(xo * rows, rows), rows)
+            send_b[i, xo] = (keep[i, at, :] + recv_a[i, at, :].astype(f32)).astype(bf16)
+            copy_b(i, xo).start()
+        at = pl.ds(pl.multiple_of(x * rows, rows), rows)
+        own[i] = keep[i, at, :] + recv_a[i, at, :].astype(f32)
+
+    def stage_c(i):
+        for xo in others_x:
+            copy_b_in(i, xo).wait_recv()
+        total = own[i]
+        for xo in others_x:
+            total = total + recv_b[i, xo].astype(f32)
+        return total
+
+    own_copies[0].wait()
+    stage_a(S, lambda half_of: heads_v[half_of], wout)
+    stage_b(S)
+    mine = pl.ds(pl.multiple_of(x * rows, rows), rows)
+    mid_all[s, c, mine, :] = layer_scale(
+        ALPHA * res_ref[...].astype(f32) + stage_c(S), mg_ref[...]
+    ).astype(bf16)
+
+    def place(so, xo, co):
+        return mid_all.at[so, co, pl.ds(pl.multiple_of(xo * rows, rows), rows), :]
+
+    def mid_z(to):
+        return remote(place(s, x, c), place(s, x, c), z_s.at[to], z_r.at[s], sp=to)
+
+    def mid_z_in(so):
+        return remote(place(so, x, c), place(so, x, c), z_s.at[so], z_r.at[so], sp=so)
+
+    def mid_x(so, xo):
+        return remote(place(so, x, c), place(so, x, c), x_s.at[so, xo], x_r.at[so, x], tp=at_x(xo))
+
+    def mid_x_in(so, xo):
+        return remote(
+            place(so, xo, c), place(so, xo, c), x_s.at[so, xo], x_r.at[so, xo], tp=at_x(xo)
+        )
+
+    def mid_d(so, xo):
+        return remote(place(so, xo, c), place(so, xo, c), d_s.at[so, xo], d_r.at[so, xo], tp=mate)
+
+    def mid_d_in(so, xo):
+        return remote(
+            place(so, xo, 1 - c), place(so, xo, 1 - c), d_s.at[so, xo], d_r.at[so, xo], tp=mate
+        )
+
+    for so in others_s:
+        mid_z(so).start()
+    for xo in others_x:
+        mid_x(s, xo).start()
+    mid_d(s, x).start()
+    forward_weight(0)
+
+    def spread(so):
+        mid_z_in(so).wait_recv()
+        for xo in others_x:
+            mid_x(so, xo).start()
+        mid_d(so, x).start()
+
+    def lift(k, carry):
+        so = lax.rem(s + k, S)
+
+        @pl.when(k + 1 < S)
+        def _():
+            spread(lax.rem(s + k + 1, S))
+
+        for xo in others_x:
+            mid_x_in(so, xo).wait_recv()
+            mid_d(so, xo).start()
+        for xo in range(X):
+            mid_d_in(so, xo).wait_recv()
+
+        @pl.when(k == 0)
+        def _():
+            finish_weight(0)
+            own_copies[1].wait()
+
+        for co in range(2):
+            up = jnp.dot(mid_all[so, co], wup[...], preferred_element_type=f32)
+            act[so, co] = jnp.square(jnp.maximum(up, 0.0)).astype(bf16)
+        return carry
+
+    lax.fori_loop(0, S, lift, 0)
+    forward_weight(1)
+    own_copies[2].wait()
+    finish_weight(1)
+
+    def copy_c(to):
+        return remote(send_c.at[to], recv_c.at[s], c_s.at[to], c_r.at[s], sp=to)
+
+    def copy_c_in(so):
+        return remote(send_c.at[so], recv_c.at[so], c_s.at[so], c_r.at[so], sp=so)
+
+    def lower(k, carry):
+        @pl.when(k < S)
+        def _():
+            so = lax.rem(s + 1 + k, S)
+            stage_a(so, lambda half_of: act[so, half_of], wdn)
+
+        @pl.when(jnp.logical_and(k >= 1, k <= S))
+        def _():
+            stage_b(lax.rem(s + k, S))
+
+        @pl.when(jnp.logical_and(k >= 2, k <= S))
+        def _():
+            so = lax.rem(s + k - 1, S)
+            send_c[so] = stage_c(so).astype(bf16)
+            copy_c(so).start()
+
+        return carry
+
+    lax.fori_loop(0, S + 1, lower, 0)
+    total = stage_c(s)
+    for so in others_s:
+        copy_c_in(so).wait_recv()
+        total = total + recv_c[so].astype(f32)
+    out_ref[...] = layer_scale(
+        ALPHA * mid_all[s, c, mine, :].astype(f32) + total, cg_ref[...]
+    ).astype(bf16)
+
+    for d in range(1, S):
+
+        @pl.when(s + d < S)
+        def _(d=d):
+            for copy in kv_copies(d):
+                copy.wait_send()
+
+    for so in others_s:
+        for m in range(2):
+            z_weight(m, so).wait_send()
+            for go in others_g:
+                y_weight(m, so, go).wait_send()
+        mid_z(so).wait_send()
+        copy_c(so).wait_send()
+
+    def drain_mid(so, carry):
+        for xo in others_x:
+            mid_x(so, xo).wait_send()
+        for xo in range(X):
+            mid_d(so, xo).wait_send()
+        return carry
+
+    lax.fori_loop(0, S, drain_mid, 0)
+
+    def drain_sums(i, carry):
+        copy_a(i).wait_send()
+        for xo in others_x:
+            copy_b(i, xo).wait_send()
+        return carry
+
+    lax.fori_loop(0, S + 1, drain_sums, 0)
+
+
+def fused_plan(G, S, T, args):
+    tok, qcols = args[1].shape
+    kcols = args[2].shape[1]
+    heads = args[4].shape[1]
+    D = args[0].shape[1]
+    ff = args[7].shape[1]
+    if S < 2 or T < 2 or T % 2 or G < 2 or tok % T or D % S or ff % S:
+        return None
+    X, rows, dcut, fcut = T // 2, tok // T, D // S, ff // S
+    if rows % 16 or dcut % 128 or fcut % 128 or D % 128 or tok % 128:
+        return None
+    if dcut % (16 * G) or fcut % (16 * G):
+        return None
+    half = X * rows
+    bf16, f32 = jnp.bfloat16, jnp.float32
+    buffers = [
+        ((S, tok, kcols), bf16),
+        ((S, tok, kcols), bf16),
+        ((S, heads, tok), f32),
+        ((qcols, D), bf16),
+        ((D, fcut), bf16),
+        ((fcut, D), bf16),
+        ((2, half, qcols), bf16),
+        ((S, 2, half, D), bf16),
+        ((S, 2, half, fcut), bf16),
+        ((S + 1, half, D), bf16),
+        ((S + 1, half, D), bf16),
+        ((S + 1, half, D), f32),
+        ((S + 1, X, rows, D), bf16),
+        ((S + 1, X, rows, D), bf16),
+        ((S + 1, rows, D), f32),
+        ((S, rows, D), bf16),
+        ((S, rows, D), bf16),
+        ((heads, tok, HD), f32),
+        ((heads, tok, HD), f32),
+        ((heads, tok, HD), f32),
+    ]
+    total = 0
+    for shape, kind in buffers:
+        size = jnp.dtype(kind).itemsize
+        for extent in shape:
+            size *= extent
+        total += size
+    if total > 48 * 2**20:
+        return None
+    sems = [
+        (S, 3),
+        (S, 3),
+        (2, S),
+        (2, S),
+        (2, S, G),
+        (2, S, G),
+        (3,),
+        (S,),
+        (S,),
+        (S, X),
+        (S, X),
+        (S, X),
+        (S, X),
+        (S + 1,),
+        (S + 1,),
+        (S + 1, X),
+        (S + 1, X),
+        (S,),
+        (S,),
+    ]
+    return [pltpu.VMEM(shape, kind) for shape, kind in buffers] + [
+        pltpu.SemaphoreType.DMA(shape) for shape in sems
+    ]
+
+
+def fused(sizes, *args):
+    scratch = fused_plan(*sizes, args)
+    if scratch is None:
+        return shards(*args)
+    res, q, k, v, gate, hg, w_out, w_up, w_down, mg, cg = args
+    vmem = pl.BlockSpec(memory_space=pltpu.VMEM)
+    hbm = pl.BlockSpec(memory_space=pl.ANY)
+    return pl.pallas_call(
+        functools.partial(layer_kernel, *sizes),
+        out_shape=jax.ShapeDtypeStruct(res.shape, jnp.bfloat16),
+        in_specs=[vmem] * 9 + [hbm] * 3,
+        out_specs=vmem,
+        scratch_shapes=scratch,
+        compiler_params=pltpu.CompilerParams(
+            collective_id=0, has_side_effects=True, vmem_limit_bytes=60 * 2**20
+        ),
+        name="layer",
+    )(q, k, v, gate, gate.T, res, hg[None], mg[None], cg[None], w_out, w_up, w_down)
+
+
 def solution(mesh):
     placed = (
         P(("grp", "sp", "tp"), None),
@@ -157,6 +687,7 @@
         P(),
         P(),
     )
+    sizes = (mesh.shape["grp"], mesh.shape["sp"], mesh.shape["tp"])
     return jax.shard_map(
-        shards, mesh=mesh, in_specs=placed, out_specs=P(("grp", "sp", "tp"), None), check_vma=False
-    )
+        functools.partial(fused, sizes), mesh=mesh, in_specs=placed, out_specs=P(("grp", "sp", "tp"), None), check_vma=False
+    )

time: 452 us -> 150 us (0.33)
  waiting for transfers between devices: 366 us -> 0 us
  Pallas kernels: 0 us -> 145 us
  blocking collectives: 44.2 us -> 0 us
  matrix products: 17.5 us -> 0 us
  between operations: 13.3 us -> 0.01 us
  other arithmetic: 10.1 us -> 0 us
    all_gather x3 -> x0, waiting for transfers between devices: 316 us -> none  [the longest x1 151 us: shards(): lax.all_gather(w_up, 'sp', axis=0, tiled=True)]
    pallas_call x0 -> x1, Pallas kernels: none -> 145 us  [fused(): pl.pallas_call(functools.partial(layer_kernel, *sizes), out_shape=jax.Sha...]
    reduce_scatter x2 -> x0, waiting for transfers between devices: 48.9 us -> none  [the longest x1 25.8 us: shards(): lax.psum_scatter(jnp.dot(heads_out, w_out, preferred_element_type=jnp.flo...]
    all_gather x3 -> x0, blocking collectives: 44.2 us -> none  [the longest x1 16 us: shards(): lax.all_gather(key_rows, 'sp', axis=0, tiled=True)]
    dot_general x4 -> x0, matrix products: 17.5 us -> none  [the longest x1 11.6 us: shards(): jnp.dot(active, down_full, preferred_element_type=jnp.float32)]
    reduce_sum x6 -> x0, other arithmetic: 6.17 us -> none  [the longest x2 2.35 us: layer_scale(): variance = jnp.mean(centered * centered, axis=-1, keepdims=True)]
  transfers between devices with their start and end apart: 5 -> 0, of which waited for: 5 -> 0; matrix products, arithmetic and copies ran while one was open for 0% -> 0% of each run, Pallas kernels for 0% -> 0%
where the time goes in v1:
time: 150 us; the launch traced here: 148 us
  Pallas kernels  145 us (97%)
  local copies, waits for them, and re-layouts  3.15 us (2%)
    pallas_call x1, Pallas kernels, fused(): pl.pallas_call(functools.partial(layer_kernel, *sizes), out_shape=jax.Sha...  145 us
    unnamed x2, local copies, waits for them, and re-layouts  3.15 us

profile of v1, /device:TPU:0, one launch (start us, length us, event | category | flops | bytes accessed | tf_op | source)
XLA Modules:
  0.0 147.9 jit_solution(5868296597230001047)
XLA Ops:
  0.0 1.5 %copy.12.gq_ref = f32[256,4]{1,0:T(8,128)} copy(f32[256,4]{0,1:T(4,128)} %param.15) | data formatting | bytes 8192 | tf_op args[4]
  1.5 144.7 %layer.1 = bf16[64,2048]{1,0:T(8,128)(2,1)} custom-call(bf16[256,512]{1,0:T(8,128)(2,1)} %q_ref.1, bf16[256,128]{1,0:T(8,128)(2,1)} %k_ref.1, bf16[256,128]{1,0:T(8,128)(2,1)} %v_ref.1, f32[256,4]{1,0:T(8,128)} %copy.12.gq_ref, f32[4,256]{1,0:T(4,128)} %bitcast.4, bf16[64,2048]{1,0:T(8,128)(2,1)} %res_ref.1, f32[1,512]{1,0:T(1,128)} %bitcast.7, ...), custom_call_target="tpu_custom_call" | custom-call | tf_op jit(solution)/shard_map/layer/pallas_call | solution.py:663
  146.2 1.7 %copy.14 = bf16[64,2048]{1,0:T(8,128)(2,1)} copy(bf16[64,2048]{1,0:T(8,128)(2,1)} %layer.1) | data formatting | bytes 524288

commit v2 on v1

--- a/solution.py
+++ b/solution.py
@@ -175,6 +175,12 @@
     heads_v,
     mid_all,
     act,
+    far_out,
+    far_in,
+    far_keep,
+    far_x_out,
+    far_x_in,
+    far_own,
     send_a,
     recv_a,
     keep,
@@ -183,6 +189,7 @@
     own,
     send_c,
     recv_c,
+    total,
     st_m,
     st_l,
     st_o,
@@ -216,7 +223,6 @@
     kv_heads = k_ref.shape[1] // HD
     group = heads // kv_heads
     rows = tok // T
-    half = X * rows
     D = res_ref.shape[1]
     dcut = D // S
     fcut = wup.shape[1]
@@ -247,7 +253,7 @@
         ),
         pltpu.make_async_copy(
             wdn_hbm.at[pl.ds(pl.multiple_of(s * fcut, fcut), fcut), :],
-            wdn.at[:, pl.ds(pl.multiple_of(s * dcut, dcut), dcut)],
+            wdn.at[s],
             loc.at[2],
         ),
     ]
@@ -285,10 +291,7 @@
         return wup.at[pl.ds(pl.multiple_of(so * dcut + go * uprow, uprow), uprow), :]
 
     def dn_piece(so, go):
-        return wdn.at[
-            pl.ds(pl.multiple_of(go * dnrow, dnrow), dnrow),
-            pl.ds(pl.multiple_of(so * dcut, dcut), dcut),
-        ]
+        return wdn.at[so, pl.ds(pl.multiple_of(go * dnrow, dnrow), dnrow), :]
 
     def z_weight(m, to):
         if m == 0:
@@ -318,19 +321,16 @@
         for so in others_s:
             z_weight(m, so).start()
 
-    def forward_weight(m):
-        for so in others_s:
-            z_weight_in(m, so).wait_recv()
-            for go in others_g:
-                y_weight(m, so, go).start()
-
-    def finish_weight(m):
-        for so in others_s:
-            for go in others_g:
-                y_weight_in(m, so, go).wait_recv()
+    def forward_piece(m, so):
+        z_weight_in(m, so).wait_recv()
+        for go in others_g:
+            y_weight(m, so, go).start()
+
+    def finish_piece(m, so):
+        for go in others_g:
+            y_weight_in(m, so, go).wait_recv()
 
     start_weight(0)
-    start_weight(1)
 
     scale = HD ** (-0.5)
     nt = (((1,), (1,)), ((), ()))
@@ -396,68 +396,75 @@
             ]
 
     chunk = 512 if D % 512 == 0 else 128
-
-    def product(lhs, weight, put):
+    branch_bufs = (far_out, far_in, far_keep, far_x_out, far_x_in, far_own)
+
+    def sum_bufs(e):
+        return [ref.at[e] for ref in (send_a, recv_a, keep, send_b, recv_b, own)]
+
+    def copy_a(i, bufs):
+        return remote(bufs[0], bufs[1], a_s.at[i], a_r.at[i], tp=mate)
+
+    def copy_b(i, bufs, xo):
+        return remote(
+            bufs[3].at[xo], bufs[4].at[x], b_s.at[i, xo], b_r.at[i, x], tp=at_x(xo)
+        )
+
+    def copy_b_in(i, bufs, xo):
+        return remote(
+            bufs[3].at[xo], bufs[4].at[xo], b_s.at[i, xo], b_r.at[i, xo], tp=at_x(xo)
+        )
+
+    def stage_b(i, bufs):
+        copy_a(i, bufs).wait_recv()
+        near, near_x = bufs[2], bufs[1]
+        for xo in others_x:
+            bufs[3][xo] = (near[xo] + near_x[xo].astype(f32)).astype(bf16)
+            copy_b(i, bufs, xo).start()
+        bufs[5][...] = near[x] + near_x[x].astype(f32)
+
+    def stage_c(i, bufs):
+        for xo in others_x:
+            copy_b_in(i, bufs, xo).wait_recv()
+        summed = bufs[5][...]
+        for xo in others_x:
+            summed = summed + bufs[4][xo].astype(f32)
+        return summed
+
+    def branch_half(co, put):
         for n in range(0, D, chunk):
-            put(n, jnp.dot(lhs, weight[:, n : n + chunk], preferred_element_type=f32))
-
-    def copy_a(i):
-        return remote(send_a.at[i], recv_a.at[i], a_s.at[i], a_r.at[i], tp=mate)
-
-    def copy_b(i, xo):
-        return remote(
-            send_b.at[i, xo], recv_b.at[i, x], b_s.at[i, xo], b_r.at[i, x], tp=at_x(xo)
-        )
-
-    def copy_b_in(i, xo):
-        return remote(
-            send_b.at[i, xo], recv_b.at[i, xo], b_s.at[i, xo], b_r.at[i, xo], tp=at_x(xo)
-        )
-
-    def stage_a(i, lhs_of, weight):
-        def put_far(n, val):
-            send_a[i, :, n : n + chunk] = val.astype(bf16)
-
-        def put_near(n, val):
-            keep[i, :, n : n + chunk] = val
-
-        product(lhs_of(1 - c), weight, put_far)
-        copy_a(i).start()
-        product(lhs_of(c), weight, put_near)
-
-    def stage_b(i):
-        copy_a(i).wait_recv()
-        for xo in others_x:
-            at = pl.ds(pl.multiple_of(xo * rows, rows), rows)
-            send_b[i, xo] = (keep[i, at, :] + recv_a[i, at, :].astype(f32)).astype(bf16)
-            copy_b(i, xo).start()
-        at = pl.ds(pl.multiple_of(x * rows, rows), rows)
-        own[i] = keep[i, at, :] + recv_a[i, at, :].astype(f32)
-
-    def stage_c(i):
-        for xo in others_x:
-            copy_b_in(i, xo).wait_recv()
-        total = own[i]
-        for xo in others_x:
-            total = total + recv_b[i, xo].astype(f32)
-        return total
+            put(
+                n,
+                jnp.dot(heads_v[co], wout[:, n : n + chunk], preferred_element_type=f32).reshape(
+                    X, rows, chunk
+                ),
+            )
+
+    def put_far(n, val):
+        far_out[:, :, n : n + chunk] = val.astype(bf16)
+
+    def put_near(n, val):
+        far_keep[:, :, n : n + chunk] = val
 
     own_copies[0].wait()
-    stage_a(S, lambda half_of: heads_v[half_of], wout)
-    stage_b(S)
+    branch_half(1 - c, put_far)
+    copy_a(S, branch_bufs).start()
+    branch_half(c, put_near)
+    stage_b(S, branch_bufs)
     mine = pl.ds(pl.multiple_of(x * rows, rows), rows)
     mid_all[s, c, mine, :] = layer_scale(
-        ALPHA * res_ref[...].astype(f32) + stage_c(S), mg_ref[...]
+        ALPHA * res_ref[...].astype(f32) + stage_c(S, branch_bufs), mg_ref[...]
     ).astype(bf16)
 
     def place(so, xo, co):
         return mid_all.at[so, co, pl.ds(pl.multiple_of(xo * rows, rows), rows), :]
 
-    def mid_z(to):
-        return remote(place(s, x, c), place(s, x, c), z_s.at[to], z_r.at[s], sp=to)
+    def mid_z(so, way):
+        return remote(
+            place(so, x, c), place(so, x, c), z_s.at[so, way], z_r.at[so], sp=s + (1 if way else -1)
+        )
 
     def mid_z_in(so):
-        return remote(place(so, x, c), place(so, x, c), z_s.at[so], z_r.at[so], sp=so)
+        return remote(place(so, x, c), place(so, x, c), z_s.at[so, 0], z_r.at[so], sp=so)
 
     def mid_x(so, xo):
         return remote(place(so, x, c), place(so, x, c), x_s.at[so, xo], x_r.at[so, x], tp=at_x(xo))
@@ -475,78 +482,141 @@
             place(so, xo, 1 - c), place(so, xo, 1 - c), d_s.at[so, xo], d_r.at[so, xo], tp=mate
         )
 
-    for so in others_s:
-        mid_z(so).start()
+    @pl.when(s + 1 < S)
+    def _():
+        mid_z(s, 1).start()
+
+    @pl.when(s > 0)
+    def _():
+        mid_z(s, 0).start()
+
     for xo in others_x:
         mid_x(s, xo).start()
     mid_d(s, x).start()
-    forward_weight(0)
+    for so in others_s:
+        forward_piece(0, so)
 
     def spread(so):
-        mid_z_in(so).wait_recv()
         for xo in others_x:
             mid_x(so, xo).start()
         mid_d(so, x).start()
 
-    def lift(k, carry):
-        so = lax.rem(s + k, S)
-
-        @pl.when(k + 1 < S)
-        def _():
-            spread(lax.rem(s + k + 1, S))
-
+    def spread_left(so):
+        mid_z_in(so).wait_recv()
+
+        @pl.when(s + 1 < S)
+        def _():
+            mid_z(so, 1).start()
+
+        spread(so)
+
+    def spread_right(so):
+        mid_z_in(so).wait_recv()
+
+        @pl.when(s > 0)
+        def _():
+            mid_z(so, 0).start()
+
+        spread(so)
+
+    def lift_block(so):
         for xo in others_x:
             mid_x_in(so, xo).wait_recv()
             mid_d(so, xo).start()
         for xo in range(X):
             mid_d_in(so, xo).wait_recv()
-
-        @pl.when(k == 0)
-        def _():
-            finish_weight(0)
-            own_copies[1].wait()
-
+        at = pl.ds(pl.multiple_of(so * rows, rows), rows)
         for co in range(2):
             up = jnp.dot(mid_all[so, co], wup[...], preferred_element_type=f32)
-            act[so, co] = jnp.square(jnp.maximum(up, 0.0)).astype(bf16)
+            up = jnp.square(jnp.maximum(up, 0.0)).astype(bf16)
+            for xo in range(X):
+                act[co, xo, at, :] = up[xo * rows : (xo + 1) * rows]
+
+    def lift(d, carry):
+        @pl.when(d + 1 < S)
+        def _():
+            @pl.when(s - d - 1 >= 0)
+            def _():
+                spread_left(s - d - 1)
+
+            @pl.when(s + d + 1 < S)
+            def _():
+                spread_right(s + d + 1)
+
+            @pl.when(d + 1 == S - 1)
+            def _():
+                start_weight(1)
+
+        @pl.when(d == 0)
+        def _():
+            for so in others_s:
+                finish_piece(0, so)
+            own_copies[1].wait()
+
+        @pl.when(s - d >= 0)
+        def _():
+            lift_block(s - d)
+
+        @pl.when(jnp.logical_and(d > 0, s + d < S))
+        def _():
+            lift_block(s + d)
+
         return carry
 
     lax.fori_loop(0, S, lift, 0)
-    forward_weight(1)
+
+    def copy_c(e, to):
+        return remote(send_c.at[e, to], recv_c.at[e, s], c_s.at[e, to], c_r.at[e, s], sp=to)
+
+    def copy_c_in(e, so):
+        return remote(send_c.at[e, so], recv_c.at[e, so], c_s.at[e, so], c_r.at[e, so], sp=so)
+
+    def half_sum(e, co):
+        lhs = act[co].reshape(X * S * rows, fcut)
+        return jnp.dot(lhs, wdn[e], preferred_element_type=f32).reshape(X, S * rows, dcut)
+
     own_copies[2].wait()
-    finish_weight(1)
-
-    def copy_c(to):
-        return remote(send_c.at[to], recv_c.at[s], c_s.at[to], c_r.at[s], sp=to)
-
-    def copy_c_in(so):
-        return remote(send_c.at[so], recv_c.at[so], c_s.at[so], c_r.at[so], sp=so)
+    forward_piece(1, others_s[0])
 
     def lower(k, carry):
         @pl.when(k < S)
         def _():
-            so = lax.rem(s + 1 + k, S)
-            stage_a(so, lambda half_of: act[so, half_of], wdn)
-
-        @pl.when(jnp.logical_and(k >= 1, k <= S))
-        def _():
-            stage_b(lax.rem(s + k, S))
-
-        @pl.when(jnp.logical_and(k >= 2, k <= S))
-        def _():
-            so = lax.rem(s + k - 1, S)
-            send_c[so] = stage_c(so).astype(bf16)
-            copy_c(so).start()
+            e = lax.rem(s + k, S)
+            bufs = sum_bufs(e)
+            bufs[0][...] = half_sum(e, 1 - c).astype(bf16)
+            copy_a(e, bufs).start()
+            bufs[2][...] = half_sum(e, c)
+            stage_b(e, bufs)
+
+        @pl.when(k + 2 < S)
+        def _():
+            forward_piece(1, lax.rem(s + k + 2, S))
+
+        @pl.when(k >= 1)
+        def _():
+            e = lax.rem(s + k - 1, S)
+            summed = stage_c(e, sum_bufs(e))
+            own[e] = summed
+            send_c[e] = summed.astype(bf16).reshape(S, rows, dcut)
+            for so in others_s:
+                copy_c(e, so).start()
+
+        @pl.when(k + 1 < S)
+        def _():
+            finish_piece(1, lax.rem(s + k + 1, S))
 
         return carry
 
     lax.fori_loop(0, S + 1, lower, 0)
-    total = stage_c(s)
-    for so in others_s:
-        copy_c_in(so).wait_recv()
-        total = total + recv_c[so].astype(f32)
+    here = pl.ds(pl.multiple_of(s * rows, rows), rows)
+    for e in range(S):
+        summed = own[e, here, :]
+        for so in others_s:
+            copy_c_in(e, so).wait_recv()
+            summed = summed + recv_c[e, so].astype(f32)
+        total[:, e * dcut : (e + 1) * dcut] = summed
     out_ref[...] = layer_scale(
-        ALPHA * mid_all[s, c, mine, :].astype(f32) + total, cg_ref[...]
+        ALPHA * mid_all[s, c, mine, :].astype(f32) + total[...], cg_ref[...]
     ).astype(bf16)
 
     for d in range(1, S):
@@ -561,10 +631,18 @@
             z_weight(m, so).wait_send()
             for go in others_g:
                 y_weight(m, so, go).wait_send()
-        mid_z(so).wait_send()
-        copy_c(so).wait_send()
+        for e in range(S):
+            copy_c(e, so).wait_send()
 
     def drain_mid(so, carry):
+        @pl.when(jnp.logical_and(so <= s, s + 1 < S))
+        def _():
+            mid_z(so, 1).wait_send()
+
+        @pl.when(jnp.logical_and(so >= s, s > 0))
+        def _():
+            mid_z(so, 0).wait_send()
+
         for xo in others_x:
             mid_x(so, xo).wait_send()
         for xo in range(X):
@@ -573,13 +651,18 @@
 
     lax.fori_loop(0, S, drain_mid, 0)
 
-    def drain_sums(i, carry):
-        copy_a(i).wait_send()
+    copy_a(S, branch_bufs).wait_send()
+    for xo in others_x:
+        copy_b(S, branch_bufs, xo).wait_send()
+
+    def drain_sums(e, carry):
+        bufs = sum_bufs(e)
+        copy_a(e, bufs).wait_send()
         for xo in others_x:
-            copy_b(i, xo).wait_send()
+            copy_b(e, bufs, xo).wait_send()
         return carry
 
-    lax.fori_loop(0, S + 1, drain_sums, 0)
+    lax.fori_loop(0, S, drain_sums, 0)
 
 
 def fused_plan(G, S, T, args):
@@ -603,18 +686,25 @@
         ((S, heads, tok), f32),
         ((qcols, D), bf16),
         ((D, fcut), bf16),
-        ((fcut, D), bf16),
+        ((S, fcut, dcut), bf16),
         ((2, half, qcols), bf16),
         ((S, 2, half, D), bf16),
-        ((S, 2, half, fcut), bf16),
-        ((S + 1, half, D), bf16),
-        ((S + 1, half, D), bf16),
-        ((S + 1, half, D), f32),
-        ((S + 1, X, rows, D), bf16),
-        ((S + 1, X, rows, D), bf16),
-        ((S + 1, rows, D), f32),
-        ((S, rows, D), bf16),
-        ((S, rows, D), bf16),
+        ((2, X, S * rows, fcut), bf16),
+        ((X, rows, D), bf16),
+        ((X, rows, D), bf16),
+        ((X, rows, D), f32),
+        ((X, rows, D), bf16),
+        ((X, rows, D), bf16),
+        ((rows, D), f32),
+        ((S, X, S * rows, dcut), bf16),
+        ((S, X, S * rows, dcut), bf16),
+        ((S, X, S * rows, dcut), f32),
+        ((S, X, S * rows, dcut), bf16),
+        ((S, X, S * rows, dcut), bf16),
+        ((S, S * rows, dcut), f32),
+        ((S, S, rows, dcut), bf16),
+        ((S, S, rows, dcut), bf16),
+        ((rows, D), f32),
         ((heads, tok, HD), f32),
         ((heads, tok, HD), f32),
         ((heads, tok, HD), f32),
@@ -635,7 +725,7 @@
         (2, S, G),
         (2, S, G),
         (3,),
-        (S,),
+        (S, 2),
         (S,),
         (S, X),
         (S, X),
@@ -645,8 +735,8 @@
         (S + 1,),
         (S + 1, X),
         (S + 1, X),
-        (S,),
-        (S,),
+        (S, S),
+        (S, S),
     ]
     return [pltpu.VMEM(shape, kind) for shape, kind in buffers] + [
         pltpu.SemaphoreType.DMA(shape) for shape in sems

time: 150 us -> 121 us (0.81); the launches traced: 148 us -> 121 us
  Pallas kernels: 145 us -> 118 us
    pallas_call x1, Pallas kernels: 145 us -> 118 us  [fused(): pl.pallas_call(functools.partial(layer_kernel, *sizes), out_shape=jax.Sha...]
where the time goes in v2:
time: 121 us
  Pallas kernels  118 us (98%)
  local copies, waits for them, and re-layouts  3.15 us (3%)
    pallas_call x1, Pallas kernels, fused(): pl.pallas_call(functools.partial(layer_kernel, *sizes), out_shape=jax.Sha...  118 us
    unnamed x2, local copies, waits for them, and re-layouts  3.15 us

profile of v2, /device:TPU:0, one launch (start us, length us, event | category | flops | bytes accessed | tf_op | source)
XLA Modules:
  0.0 121.3 jit_solution(12607227236420260053)
XLA Ops:
  0.0 1.5 %copy.12.gq_ref = f32[256,4]{1,0:T(8,128)} copy(f32[256,4]{0,1:T(4,128)} %param.15) | data formatting | bytes 8192 | tf_op args[4]
  1.5 118.1 %layer.1 = bf16[64,2048]{1,0:T(8,128)(2,1)} custom-call(bf16[256,512]{1,0:T(8,128)(2,1)} %q_ref.1, bf16[256,128]{1,0:T(8,128)(2,1)} %k_ref.1, bf16[256,128]{1,0:T(8,128)(2,1)} %v_ref.1, f32[256,4]{1,0:T(8,128)} %copy.12.gq_ref, f32[4,256]{1,0:T(4,128)} %bitcast.4, bf16[64,2048]{1,0:T(8,128)(2,1)} %res_ref.1, f32[1,512]{1,0:T(1,128)} %bitcast.7, ...), custom_call_target="tpu_custom_call" | custom-call | tf_op jit(solution)/shard_map/layer/pallas_call | solution.py:753
  119.6 1.7 %copy.14 = bf16[64,2048]{1,0:T(8,128)(2,1)} copy(bf16[64,2048]{1,0:T(8,128)(2,1)} %layer.1) | data formatting | bytes 524288
